TPU v7x, 32 devices: a whole 2x2x4 slice. The times are simulated.
32 devices in a mesh: fs: 8 (over z, y), tp: 4 (over x, core).
Axes of the slice: x: 2, y: 2, z: 4, core: 2. Of those that a mesh axis runs over, the one named last changes fastest.
Arguments:
- tokens: bfloat16 [3072, 2048], P('fs'), may hold values from -6 to 6
- first_norm_scale: float32 [2048], replicated, may hold values from 0.1 to 1.9
- recurrent_branch_matrix: bfloat16 [2048, 1024], P('fs', 'tp'), may hold values from -0.125 to 0.125
- gelu_gate_matrix: bfloat16 [2048, 1024], P('fs', 'tp'), may hold values from -0.125 to 0.125
- filter_taps_weight: bfloat16 [4, 1024], P(None, 'tp'), may hold values from -3 to 3
- recurrence_gate_blocks: bfloat16 [16, 64, 64], P('tp'), may hold values from -0.75 to 0.75
- input_gate_blocks: bfloat16 [16, 64, 64], P('tp'), may hold values from -0.75 to 0.75
- base_decay_logits: float32 [1024], P('tp'), may hold values from 4 to 11
- extra_log_decay: float32 [3072, 1024], P('fs', 'tp'), may hold values from -0.7 to 0
- mixer_output_matrix: bfloat16 [2048, 1024], P('fs', 'tp'), may hold values from -0.5 to 0.5
- second_norm_scale: float32 [2048], replicated, may hold values from 0.1 to 1.9
- mixer_up_matrix: bfloat16 [2048, 4096], P('fs', 'tp'), may hold values from -0.125 to 0.125
- mixer_down_matrix: bfloat16 [2048, 4096], P('fs', 'tp'), may hold values from -0.09375 to 0.09375
Outputs:
- layer_out: bfloat16 [3072, 2048], P(('fs', 'tp'))
All inputs are finite; a program needn't handle non-finite values.
Results may differ from a plain program's by a relative error of at most 0.022.
Values may be sent and summed in bfloat16 or wider, within the bound.
A program may use at most 64 MiB of HBM per device.

v0:
```python
import jax
import jax.numpy as jnp
from jax import lax
from jax.sharding import PartitionSpec as P

epsilon = 1e-06
decay_rate_scale = 8.0


def rms_scaled(sequence_token_rows, scales):
    widened = sequence_token_rows.astype(jnp.float32)
    mean_square = jnp.mean(widened * widened, axis=-1, keepdims=True)
    return (widened * lax.rsqrt(mean_square + epsilon) * scales).astype(jnp.bfloat16)


def linear_combine(earlier, later):
    return (earlier[0] * later[0], later[0] * earlier[1] + later[1])


def causal_taps(branch, filter_taps_weight):
    tap_count = filter_taps_weight.shape[0]
    positions = branch.shape[0]
    padded = jnp.pad(branch.astype(jnp.float32), ((tap_count - 1, 0), (0, 0)))
    running = jnp.zeros(branch.shape, jnp.float32)
    for offset in range(tap_count):
        running = running + padded[offset : offset + positions] * filter_taps_weight[offset].astype(
            jnp.float32
        )
    return running.astype(jnp.bfloat16)


def block_map(convolved, blocks):
    positions, channels = convolved.shape
    grouped = convolved.reshape(positions, blocks.shape[0], blocks.shape[1])
    mapped = jnp.einsum("sgi,gij->sgj", grouped, blocks, preferred_element_type=jnp.float32)
    return jax.nn.sigmoid(mapped.reshape(positions, channels))


def contract_columns(left, right):
    return lax.dot_general(
        left, right, (((1,), (1,)), ((), ())), preferred_element_type=jnp.float32
    )


def local(
    tokens,
    first_norm_scale,
    recurrent_branch_matrix,
    gelu_gate_matrix,
    filter_taps_weight,
    recurrence_gate_blocks,
    input_gate_blocks,
    base_decay_logits,
    extra_log_decay,
    mixer_output_matrix,
    second_norm_scale,
    mixer_up_matrix,
    mixer_down_matrix,
):
    positions = tokens.shape[0]
    own_count = positions // lax.axis_size("tp")
    normed = rms_scaled(tokens, first_norm_scale)
    branch_sum = jnp.dot(
        normed,
        lax.all_gather(recurrent_branch_matrix, "fs", axis=0, tiled=True),
        preferred_element_type=jnp.float32,
    )
    gate_sum = jnp.dot(
        normed,
        lax.all_gather(gelu_gate_matrix, "fs", axis=0, tiled=True),
        preferred_element_type=jnp.float32,
    )
    branch = branch_sum.astype(jnp.bfloat16)
    gate_branch = gate_sum.astype(jnp.bfloat16)
    out_full = lax.all_gather(mixer_output_matrix, "fs", axis=0, tiled=True)
    convolved = causal_taps(branch, filter_taps_weight)
    recurrence_gate_value = block_map(convolved, recurrence_gate_blocks)
    admission = block_map(convolved, input_gate_blocks)
    log_keep_factor = (
        decay_rate_scale * recurrence_gate_value * jax.nn.log_sigmoid(base_decay_logits)
        + extra_log_decay
    )
    retain = jnp.exp(log_keep_factor)
    driven = jnp.sqrt(-jnp.expm1(2.0 * log_keep_factor)) * (
        admission * convolved.astype(jnp.float32)
    )
    memory = lax.associative_scan(linear_combine, (retain, driven), axis=0)[1]
    recurrent = (memory * jax.nn.gelu(gate_branch.astype(jnp.float32))).astype(jnp.bfloat16)
    up_full = lax.all_gather(mixer_up_matrix, "fs", axis=0, tiled=True)
    whole_sum = lax.psum(contract_columns(recurrent, out_full).astype(jnp.bfloat16), "tp").astype(
        jnp.float32
    )
    residual_all = (tokens.astype(jnp.float32) + whole_sum).astype(jnp.bfloat16)
    raised = jnp.dot(
        rms_scaled(residual_all, second_norm_scale), up_full, preferred_element_type=jnp.float32
    )
    hidden = jnp.square(jax.nn.relu(raised)).astype(jnp.bfloat16)
    residual = lax.dynamic_slice_in_dim(
        residual_all, lax.axis_index("tp") * own_count, own_count, 0
    )
    down_full = lax.all_gather(mixer_down_matrix, "fs", axis=0, tiled=True)
    channel_sum = lax.psum_scatter(
        contract_columns(hidden, down_full).astype(jnp.bfloat16),
        "tp",
        scatter_dimension=0,
        tiled=True,
    ).astype(jnp.float32)
    return (residual.astype(jnp.float32) + channel_sum).astype(jnp.bfloat16)


def solution(mesh):
    in_specs = (
        P("fs", None),
        P(),
        P("fs", "tp"),
        P("fs", "tp"),
        P(None, "tp"),
        P("tp", None, None),
        P("tp", None, None),
        P("tp"),
        P("fs", "tp"),
        P("fs", "tp"),
        P(),
        P("fs", "tp"),
        P("fs", "tp"),
    )
    out_specs = P(("fs", "tp"), None)
    return jax.shard_map(local, mesh=mesh, in_specs=in_specs, out_specs=out_specs, check_vma=False)
```

profile of v0, /device:TPU:0, one launch (start us, length us, event | category | flops | bytes accessed | tf_op | source)
XLA Modules:
  0.0 372.9 jit_solution(10167174261476025850)
XLA Ops:
  6.5 0.7 all-gather.6.cloned.1.call-update
  7.3 0.7 all-gather.10.cloned.1.call-update
  8.1 0.7 all-gather.8.cloned.1.call-update
  8.8 0.8 slice_convert_fusion.3
  9.6 1.8 fusion.3
  11.4 0.7 fusion.59
  12.1 40.4 %all-gather.6.cloned.1.call-done = bf16[2048,256]{1,0:T(8,128)(2,1)} async-done(((bf16[256,256]{1,0:T(8,128)(2,1)}), bf16[2048,256]{1,0:T(8,128)(2,1)}) %all-gather.6.cloned.1.call-update) | async-done | bytes 1048592 | tf_op jit(solution)/shard_map/all_gather | solution.py:65
  52.5 2.3 fusion.20
  55.2 0.3 fusion.18
  55.7 0.3 fusion.15
  56.2 0.5 fusion.49
  58.3 0.3 slice.278
  59.8 33.8 %all-gather.10.cloned.1.call-done = bf16[2048,256]{1,0:T(8,128)(2,1)} async-done(((bf16[256,256]{1,0:T(8,128)(2,1)}), bf16[2048,256]{1,0:T(8,128)(2,1)}) %all-gather.10.cloned.1.call-update) | async-done | bytes 1048592 | tf_op jit(solution)/shard_map/all_gather | solution.py:75
  93.6 41.2 %all-gather.8.cloned.1.call-done = bf16[2048,256]{1,0:T(8,128)(2,1)} async-done(((bf16[256,256]{1,0:T(8,128)(2,1)}), bf16[2048,256]{1,0:T(8,128)(2,1)}) %all-gather.8.cloned.1.call-update) | async-done | bytes 1048592 | tf_op jit(solution)/shard_map/all_gather | solution.py:70
  134.8 4.6 %convolution_convert_fusion.1 = bf16[384,2048]{1,0:T(8,128)(2,1)} fusion(bf16[2048,256]{1,0:T(8,128)(2,1)} %all-gather.10.cloned.1.call-done, bf16[2048,256]{1,0:T(8,128)(2,1)} %all-gather.8.cloned.1.call-done, bf16[384,2048]{1,0:T(8,128)(2,1)S(1)} %copy-done.1, f32[2048]{0:T(1024)S(1)} %copy-done.4, f32[384]{0:T(512)S(1)} %add_rsqrt_fusion.1, ...), kind=kOutput, calls=%fused_computation.13 | convolution fusion | flops 810516480 | bytes 6039040 | tf_op jit(solution)/shard_map/dot_general | solution.py:40
  139.5 0.5 all-gather.12.cloned.1.call-update
  140.1 0.5 all-gather.14.cloned.1.call-update
  140.7 40.5 %all-reduce.19.cloned.1.call-done = bf16[384,2048]{1,0:T(8,128)(2,1)} async-done(((bf16[384,2048]{1,0:T(8,128)(2,1)}), bf16[384,2048]{1,0:T(8,128)(2,1)}) %all-reduce.19.cloned.1.call-update) | async-done | bytes 1572880 | tf_op jit(solution)/shard_map/psum | solution.py:90
  181.2 2.1 fusion
  183.3 72.7 %all-gather.12.cloned.1.call-done = bf16[2048,1024]{1,0:T(8,128)(2,1)} async-done(((bf16[256,1024]{1,0:T(8,128)(2,1)}), bf16[2048,1024]{1,0:T(8,128)(2,1)}) %all-gather.12.cloned.1.call-update) | async-done | bytes 4194320 | tf_op jit(solution)/shard_map/all_gather | solution.py:89
  256.0 73.3 %all-gather.14.cloned.1.call-done = bf16[2048,1024]{1,0:T(8,128)(2,1)} async-done(((bf16[256,1024]{1,0:T(8,128)(2,1)}), bf16[2048,1024]{1,0:T(8,128)(2,1)}) %all-gather.14.cloned.1.call-update) | async-done | bytes 4194320 | tf_op jit(solution)/shard_map/all_gather | solution.py:101
  329.4 8.1 %convolution_convert_fusion = bf16[384,2048]{1,0:T(8,128)(2,1)} fusion(bf16[2048,1024]{1,0:T(8,128)(2,1)} %all-gather.14.cloned.1.call-done, bf16[2048,1024]{1,0:T(8,128)(2,1)} %all-gather.12.cloned.1.call-done, bf16[384,2048]{1,0:T(8,128)(2,1)S(1)} %get-tuple-element.6, f32[2048]{0:T(1024)S(1)} %copy-done.5, f32[384]{0:T(512)S(1)} %add_rsqrt_fusion), kind=kOutput, calls=%fused_computation.12 | convolution fusion | flops 3226337280 | bytes 11544064 | tf_op jit(solution)/shard_map/dot_general | solution.py:40
  337.6 26.7 %reduce-scatter.2.cloned.1.call-done = bf16[96,2048]{1,0:T(8,128)(2,1)} async-done(((bf16[384,2048]{1,0:T(8,128)(2,1)}), bf16[96,2048]{1,0:T(8,128)(2,1)}) %reduce-scatter.2.cloned.1.call-update) | async-done | bytes 393232 | tf_op jit(solution)/shard_map/reduce_scatter | solution.py:102
  364.2 1.8 add_convert_fusion
  (120 shorter events, 3.3 us)
Async XLA Ops:
  6.5 48.7 %copy-start = (bf16[4,64,64]{2,1,0:T(8,128)(2,1)S(1)}, bf16[4,64,64]{2,1,0:T(8,128)(2,1)}, u32[]{:S(2)}) copy-start(bf16[4,64,64]{2,1,0:T(8,128)(2,1)} %param.18) | copy-start | bytes 98308
  6.5 46.0 %all-gather.6.cloned.1.call-start = ((), (), s32[]{:S(2)}) async-start(), calls=%async_computation.1 | async-start | bytes 1179648 | tf_op jit(solution)/shard_map/all_gather | solution.py:65
  7.3 86.4 %all-gather.10.cloned.1.call-start = ((), (), s32[]{:S(2)}) async-start(), calls=%async_computation.3 | async-start | bytes 1179648 | tf_op jit(solution)/shard_map/all_gather | solution.py:75
  8.0 126.8 %all-gather.8.cloned.1.call-start = ((), (), s32[]{:S(2)}) async-start(), calls=%async_computation.2 | async-start | bytes 1179648 | tf_op jit(solution)/shard_map/all_gather | solution.py:70
  8.7 172.4 %all-reduce.19.cloned.1.call-start = ((), (), s32[]{:S(2)}) async-start(), calls=%async_computation.4 | async-start | bytes 3145728 | tf_op jit(solution)/shard_map/psum | solution.py:90
  12.1 43.6 %copy-start.3 = (bf16[4,64,64]{2,1,0:T(8,128)(2,1)S(1)}, bf16[4,64,64]{2,1,0:T(8,128)(2,1)}, u32[]{:S(2)}) copy-start(bf16[4,64,64]{2,1,0:T(8,128)(2,1)} %param.19) | copy-start | bytes 98308
  54.8 1.4 copy-start.2
  59.1 75.7 %copy-start.1 = (bf16[384,2048]{1,0:T(8,128)(2,1)S(1)}, bf16[384,2048]{1,0:T(8,128)(2,1)}, u32[]{:S(2)}) copy-start(bf16[384,2048]{1,0:T(8,128)(2,1)} %param.13) | copy-start | bytes 4718596
  59.1 75.7 %copy-start.4 = (f32[2048]{0:T(1024)S(1)}, f32[2048]{0:T(1024)}, u32[]{:S(2)}) copy-start(f32[2048]{0:T(1024)} %param.14) | copy-start | bytes 24580
  139.5 189.9 %copy-start.5 = (f32[2048]{0:T(1024)S(1)}, f32[2048]{0:T(1024)}, u32[]{:S(2)}) copy-start(f32[2048]{0:T(1024)} %param.23) | copy-start | bytes 24580
  139.5 116.6 %all-gather.12.cloned.1.call-start = ((), (), s32[]{:S(2)}) async-start(), calls=%async_computation.5 | async-start | bytes 4718592 | tf_op jit(solution)/shard_map/all_gather | solution.py:89
  140.1 189.3 %all-gather.14.cloned.1.call-start = ((), (), s32[]{:S(2)}) async-start(), calls=%async_computation.6 | async-start | bytes 4718592 | tf_op jit(solution)/shard_map/all_gather | solution.py:101
  140.6 223.6 %reduce-scatter.2.cloned.1.call-start = ((), (), s32[]{:S(2)}) async-start(), calls=%async_computation.7 | async-start | bytes 1966080 | tf_op jit(solution)/shard_map/reduce_scatter | solution.py:102
Sparse Core Ops, SparseCore 0:
  9.5 42.9 all-gather.5
  54.6 38.9 all-gather.9
  95.8 38.9 all-gather.7
  139.6 41.5 all-reduce.18
  183.2 72.8 all-gather.11
  258.0 71.3 all-gather.13
  337.7 26.5 reduce-scatter.1
where the time goes:
time: 373 us
  waiting for transfers between devices  332 us (89%)
  matrix products  15.7 us (4%)
  between operations  14.1 us (4%)
  other arithmetic  8.42 us (2%)
    all_gather x1, waiting for transfers between devices, local(): down_full = lax.all_gather(mixer_down_matrix, 'fs', axis=0, tiled=True)  73.3 us
    all_gather x1, waiting for transfers between devices, local(): up_full = lax.all_gather(mixer_up_matrix, 'fs', axis=0, tiled=True)  72.7 us
    all_gather x1, waiting for transfers between devices, local(): lax.all_gather(gelu_gate_matrix, 'fs', axis=0, tiled=True)  41.2 us
    psum x1, waiting for transfers between devices, local(): lax.psum(contract_columns(recurrent, out_full).astype(jnp.bfloat16), 'tp')  40.5 us
    all_gather x1, waiting for transfers between devices, local(): lax.all_gather(recurrent_branch_matrix, 'fs', axis=0, tiled=True)  40.4 us
    all_gather x1, waiting for transfers between devices, local(): out_full = lax.all_gather(mixer_output_matrix, 'fs', axis=0, tiled=True)  33.8 us
    reduce_scatter x1, waiting for transfers between devices, local(): lax.psum_scatter(contract_columns(hidden, down_full).astype(jnp.bfloat16)...  26.7 us
    dot_general x2, matrix products, contract_columns(): lax.dot_general(left, right, (((1,), (1,)), ((), ())), preferred_element_...  12.8 us
  transfers between devices with their start and end apart: 7, of which 7 were waited for; matrix products, arithmetic and copies ran while one was open for 3% of the time, Pallas kernels for 0%

commit v1 on v0

--- a/solution.py
+++ b/solution.py
@@ -1,3 +1,4 @@
+import functools
 import jax
 import jax.numpy as jnp
 from jax import lax
@@ -5,6 +6,21 @@
 
 epsilon = 1e-06
 decay_rate_scale = 8.0
+
+
+def lift_flows(obj, mesh_ax, dimension_no):
+    num = lax.axis_size(mesh_ax)
+    pile = [(tick, (tick + 1) % num) for tick in range(num)]
+    outcome_arr = [None] * num
+    outcome_arr[num - 1] = obj
+    for to_i in range(num - 2, -1, -1):
+        outcome_arr[to_i] = lax.ppermute(outcome_arr[to_i + 1], mesh_ax, pile)
+    frame_out = jnp.concatenate(outcome_arr, axis=dimension_no)
+    met_up = (lax.axis_index(mesh_ax) + 1) * obj.shape[dimension_no]
+    return jnp.roll(frame_out, met_up, dimension_no)
+
+
+store_loads = functools.partial(lift_flows, mesh_ax="fs", dimension_no=0)
 
 
 def rms_scaled(sequence_token_rows, scales):
@@ -72,7 +88,7 @@
     )
     branch = branch_sum.astype(jnp.bfloat16)
     gate_branch = gate_sum.astype(jnp.bfloat16)
-    out_full = lax.all_gather(mixer_output_matrix, "fs", axis=0, tiled=True)
+    out_full = store_loads(mixer_output_matrix)
     convolved = causal_taps(branch, filter_taps_weight)
     recurrence_gate_value = block_map(convolved, recurrence_gate_blocks)
     admission = block_map(convolved, input_gate_blocks)

time: 373 us -> 335 us (0.90)
  waiting for transfers between devices: 332 us -> 277 us
  local copies, waits for them, and re-layouts: 2.7 us -> 14.7 us
    ppermute x0 -> x7, waiting for transfers between devices: none -> 52.1 us  [lift_flows(): outcome_arr[to_i] = lax.ppermute(outcome_arr[to_i + 1], mesh_ax, pile)]
    all_gather x1, waiting for transfers between devices: 40.4 us -> 0.01 us  [local(): lax.all_gather(recurrent_branch_matrix, 'fs', axis=0, tiled=True)]
    all_gather x1 -> x0, waiting for transfers between devices: 33.8 us -> none  [local(): out_full = lax.all_gather(mixer_output_matrix, 'fs', axis=0, tiled=True)]
    all_gather x1, waiting for transfers between devices: 41.2 us -> 9.51 us  [local(): lax.all_gather(gelu_gate_matrix, 'fs', axis=0, tiled=True)]
    unnamed x12 -> x27, local copies, waits for them, and re-layouts: 0.03 us -> 9.96 us
  transfers between devices with their start and end apart: 7 -> 13, of which waited for: 7 -> 12; matrix products, arithmetic and copies ran while one was open for 3% -> 8% of each run, Pallas kernels for 0% -> 0%
where the time goes in v1:
time: 335 us; the launch traced here: 334 us
  waiting for transfers between devices  277 us (83%)
  matrix products  15.2 us (5%)
  local copies, waits for them, and re-layouts  14.7 us (4%)
  between operations  14.1 us (4%)
  other arithmetic  10.4 us (3%)
    all_gather x1, waiting for transfers between devices, local(): up_full = lax.all_gather(mixer_up_matrix, 'fs', axis=0, tiled=True)  73.3 us
    all_gather x1, waiting for transfers between devices, local(): down_full = lax.all_gather(mixer_down_matrix, 'fs', axis=0, tiled=True)  72.7 us
    ppermute x7, waiting for transfers between devices, lift_flows(): outcome_arr[to_i] = lax.ppermute(outcome_arr[to_i + 1], mesh_ax, pile)  52.1 us
    psum x1, waiting for transfers between devices, local(): lax.psum(contract_columns(recurrent, out_full).astype(jnp.bfloat16), 'tp')  40.5 us
    reduce_scatter x1, waiting for transfers between devices, local(): lax.psum_scatter(contract_columns(hidden, down_full).astype(jnp.bfloat16)...  26.7 us
    dot_general x2, matrix products, contract_columns(): lax.dot_general(left, right, (((1,), (1,)), ((), ())), preferred_element_...  12.7 us
    unnamed x27, local copies, waits for them, and re-layouts  9.96 us
    all_gather x1, waiting for transfers between devices, local(): lax.all_gather(gelu_gate_matrix, 'fs', axis=0, tiled=True)  9.51 us
  transfers between devices with their start and end apart: 13, of which 12 were waited for; matrix products, arithmetic and copies ran while one was open for 8% of the time, Pallas kernels for 0%

profile of v1, /device:TPU:0, one launch (start us, length us, event | category | flops | bytes accessed | tf_op | source)
XLA Modules:
  0.0 334.3 jit_solution(12055099338860707008)
XLA Ops:
  7.3 3.0 collective-permute-start
  10.4 6.7 %collective-permute-done = bf16[256,256]{1,0:T(8,128)(2,1)S(1)} collective-permute-done((bf16[256,256]{1,0:T(8,128)(2,1)}, bf16[256,256]{1,0:T(8,128)(2,1)S(1)}, u32[]{:S(2)}, u32[]{:S(2)}) %collective-permute-start) | collective-permute-done | bytes 131104 | tf_op jit(solution)/shard_map/ppermute | solution.py:17
  17.1 7.8 %collective-permute-done.1 = bf16[256,256]{1,0:T(8,128)(2,1)S(1)} collective-permute-done((bf16[256,256]{1,0:T(8,128)(2,1)S(1)}, bf16[256,256]{1,0:T(8,128)(2,1)S(1)}, u32[]{:S(2)}, u32[]{:S(2)}) %collective-permute-start.1) | collective-permute-done | bytes 131104 | tf_op jit(solution)/shard_map/ppermute | solution.py:17
  25.0 8.2 %collective-permute-done.2 = bf16[256,256]{1,0:T(8,128)(2,1)S(1)} collective-permute-done((bf16[256,256]{1,0:T(8,128)(2,1)S(1)}, bf16[256,256]{1,0:T(8,128)(2,1)S(1)}, u32[]{:S(2)}, u32[]{:S(2)}) %collective-permute-start.2) | collective-permute-done | bytes 131104 | tf_op jit(solution)/shard_map/ppermute | solution.py:17
  33.1 0.8 slice_convert_fusion.3
  34.0 6.9 %collective-permute-done.3 = bf16[256,256]{1,0:T(8,128)(2,1)S(1)} collective-permute-done((bf16[256,256]{1,0:T(8,128)(2,1)S(1)}, bf16[256,256]{1,0:T(8,128)(2,1)S(1)}, u32[]{:S(2)}, u32[]{:S(2)}) %collective-permute-start.3) | collective-permute-done | bytes 131104 | tf_op jit(solution)/shard_map/ppermute | solution.py:17
  40.9 1.8 fusion.3
  42.7 7.9 %collective-permute-done.4 = bf16[256,256]{1,0:T(8,128)(2,1)S(1)} collective-permute-done((bf16[256,256]{1,0:T(8,128)(2,1)S(1)}, bf16[256,256]{1,0:T(8,128)(2,1)S(1)}, u32[]{:S(2)}, u32[]{:S(2)}) %collective-permute-start.4) | collective-permute-done | bytes 131104 | tf_op jit(solution)/shard_map/ppermute | solution.py:17
  50.6 7.7 %collective-permute-done.5 = bf16[256,256]{1,0:T(8,128)(2,1)S(1)} collective-permute-done((bf16[256,256]{1,0:T(8,128)(2,1)S(1)}, bf16[256,256]{1,0:T(8,128)(2,1)S(1)}, u32[]{:S(2)}, u32[]{:S(2)}) %collective-permute-start.5) | collective-permute-done | bytes 131104 | tf_op jit(solution)/shard_map/ppermute | solution.py:17
  58.9 7.0 %collective-permute-done.6 = bf16[256,256]{1,0:T(8,128)(2,1)S(1)} collective-permute-done((bf16[256,256]{1,0:T(8,128)(2,1)S(1)}, bf16[256,256]{1,0:T(8,128)(2,1)S(1)}, u32[]{:S(2)}, u32[]{:S(2)}) %collective-permute-start.6) | collective-permute-done | bytes 131104 | tf_op jit(solution)/shard_map/ppermute | solution.py:17
  76.5 1.8 fusion.20
  79.6 0.9 copy.24
  80.5 1.6 fusion.50
  82.5 0.7 slice.224
  83.2 1.0 fusion.68
  86.7 9.5 %all-gather.7.cloned.1.call-done = bf16[2048,256]{1,0:T(8,128)(2,1)} async-done(((bf16[256,256]{1,0:T(8,128)(2,1)}), bf16[2048,256]{1,0:T(8,128)(2,1)}) %all-gather.7.cloned.1.call-update) | async-done | bytes 1048592 | tf_op jit(solution)/shard_map/all_gather | solution.py:86
  96.2 4.6 %convolution_convert_fusion.1 = bf16[384,2048]{1,0:T(8,128)(2,1)} fusion(bf16[4096,256]{1,0:T(8,128)(2,1)} %constant_dynamic-update-slice_fusion, s32[]{:T(128)S(6)} %select_n.23, bf16[2048,256]{1,0:T(8,128)(2,1)} %all-gather.7.cloned.1.call-done, bf16[384,2048]{1,0:T(8,128)(2,1)S(1)} %copy-done.1, f32[2048]{0:T(1024)S(1)} %copy-done.4, ...), kind=kOutput, calls=%fused_computation.13 | convolution fusion | flops 810516480 | bytes 6039044 | tf_op jit(solution)/shard_map/dot_general | solution.py:56
  102.0 40.5 %all-reduce.19.cloned.1.call-done = bf16[384,2048]{1,0:T(8,128)(2,1)} async-done(((bf16[384,2048]{1,0:T(8,128)(2,1)}), bf16[384,2048]{1,0:T(8,128)(2,1)}) %all-reduce.19.cloned.1.call-update) | async-done | bytes 1572880 | tf_op jit(solution)/shard_map/psum | solution.py:106
  142.5 2.1 fusion
  144.7 72.7 %all-gather.11.cloned.1.call-done = bf16[2048,1024]{1,0:T(8,128)(2,1)} async-done(((bf16[256,1024]{1,0:T(8,128)(2,1)}), bf16[2048,1024]{1,0:T(8,128)(2,1)}) %all-gather.11.cloned.1.call-update) | async-done | bytes 4194320 | tf_op jit(solution)/shard_map/all_gather | solution.py:117
  217.4 73.3 %all-gather.9.cloned.1.call-done = bf16[2048,1024]{1,0:T(8,128)(2,1)} async-done(((bf16[256,1024]{1,0:T(8,128)(2,1)}), bf16[2048,1024]{1,0:T(8,128)(2,1)}) %all-gather.9.cloned.1.call-update) | async-done | bytes 4194320 | tf_op jit(solution)/shard_map/all_gather | solution.py:105
  290.8 8.1 %convolution_convert_fusion = bf16[384,2048]{1,0:T(8,128)(2,1)} fusion(bf16[2048,1024]{1,0:T(8,128)(2,1)} %all-gather.11.cloned.1.call-done, bf16[2048,1024]{1,0:T(8,128)(2,1)} %all-gather.9.cloned.1.call-done, bf16[384,2048]{1,0:T(8,128)(2,1)S(1)} %get-tuple-element.6, f32[2048]{0:T(1024)S(1)} %copy-done.5, f32[384]{0:T(512)S(1)} %add_rsqrt_fusion), kind=kOutput, calls=%fused_computation.12 | convolution fusion | flops 3226337280 | bytes 11544064 | tf_op jit(solution)/shard_map/dot_general | solution.py:56
  298.9 26.7 %reduce-scatter.2.cloned.1.call-done = bf16[96,2048]{1,0:T(8,128)(2,1)} async-done(((bf16[384,2048]{1,0:T(8,128)(2,1)}), bf16[96,2048]{1,0:T(8,128)(2,1)}) %reduce-scatter.2.cloned.1.call-update) | async-done | bytes 393232 | tf_op jit(solution)/shard_map/reduce_scatter | solution.py:118
  325.6 1.8 add_convert_fusion
  (147 shorter events, 16.9 us)
Async XLA Ops:
  6.5 72.2 %copy-start = (bf16[4,64,64]{2,1,0:T(8,128)(2,1)S(1)}, bf16[4,64,64]{2,1,0:T(8,128)(2,1)}, u32[]{:S(2)}) copy-start(bf16[4,64,64]{2,1,0:T(8,128)(2,1)} %param.18) | copy-start | bytes 98308
  6.5 64.0 %copy-start.2 = (bf16[256,256]{1,0:T(8,128)(2,1)S(1)}, bf16[256,256]{1,0:T(8,128)(2,1)}, u32[]{:S(2)}) copy-start(bf16[256,256]{1,0:T(8,128)(2,1)} %param.22) | copy-start | bytes 393220
  6.5 70.0 %all-gather.5.cloned.1.call-start = ((), (), s32[]{:S(2)}) async-start(), calls=%async_computation.1 | async-start | bytes 1179648 | tf_op jit(solution)/shard_map/all_gather | solution.py:81
  7.3 88.9 %all-gather.7.cloned.1.call-start = ((), (), s32[]{:S(2)}) async-start(), calls=%async_computation.2 | async-start | bytes 1179648 | tf_op jit(solution)/shard_map/all_gather | solution.py:86
  7.3 9.8 %collective-permute-start = (bf16[256,256]{1,0:T(8,128)(2,1)}, bf16[256,256]{1,0:T(8,128)(2,1)S(1)}, u32[]{:S(2)}, u32[]{:S(2)}) collective-permute-start(bf16[256,256]{1,0:T(8,128)(2,1)} %param.22), channel_id=1, source_target_pairs={{0,4},{4,8},{8,12},{12,16},{16,20},{20,24},{24,28},{28,0},{1,5},{5... | collective-permute-start | bytes 393224 | tf_op jit(solution)/shard_map/ppermute | solution.py:17
  17.1 7.8 %collective-permute-start.1 = (bf16[256,256]{1,0:T(8,128)(2,1)S(1)}, bf16[256,256]{1,0:T(8,128)(2,1)S(1)}, u32[]{:S(2)}, u32[]{:S(2)}) collective-permute-start(bf16[256,256]{1,0:T(8,128)(2,1)S(1)} %collective-permute-done), channel_id=1, source_target_pairs={{0,4},{4,8},{8,12},{12,16},{16,20},{20,24},{24,28},{28,0},{1,5},{5... | collective-permute-start | bytes 393224 | tf_op jit(solution)/shard_map/ppermute | solution.py:17
  24.9 8.3 %collective-permute-start.2 = (bf16[256,256]{1,0:T(8,128)(2,1)S(1)}, bf16[256,256]{1,0:T(8,128)(2,1)S(1)}, u32[]{:S(2)}, u32[]{:S(2)}) collective-permute-start(bf16[256,256]{1,0:T(8,128)(2,1)S(1)} %collective-permute-done.1), channel_id=1, source_target_pairs={{0,4},{4,8},{8,12},{12,16},{16,20},{20,24},{24,28},{28,0},{1,5},{5... | collective-permute-start | bytes 393224 | tf_op jit(solution)/shard_map/ppermute | solution.py:17
  24.9 117.7 %all-reduce.19.cloned.1.call-start = ((), (), s32[]{:S(2)}) async-start(), calls=%async_computation.3 | async-start | bytes 3145728 | tf_op jit(solution)/shard_map/psum | solution.py:106
  33.1 7.8 %collective-permute-start.3 = (bf16[256,256]{1,0:T(8,128)(2,1)S(1)}, bf16[256,256]{1,0:T(8,128)(2,1)S(1)}, u32[]{:S(2)}, u32[]{:S(2)}) collective-permute-start(bf16[256,256]{1,0:T(8,128)(2,1)S(1)} %collective-permute-done.2), channel_id=1, source_target_pairs={{0,4},{4,8},{8,12},{12,16},{16,20},{20,24},{24,28},{28,0},{1,5},{5... | collective-permute-start | bytes 393224 | tf_op jit(solution)/shard_map/ppermute | solution.py:17
  40.9 9.7 %collective-permute-start.4 = (bf16[256,256]{1,0:T(8,128)(2,1)S(1)}, bf16[256,256]{1,0:T(8,128)(2,1)S(1)}, u32[]{:S(2)}, u32[]{:S(2)}) collective-permute-start(bf16[256,256]{1,0:T(8,128)(2,1)S(1)} %collective-permute-done.3), channel_id=1, source_target_pairs={{0,4},{4,8},{8,12},{12,16},{16,20},{20,24},{24,28},{28,0},{1,5},{5... | collective-permute-start | bytes 393224 | tf_op jit(solution)/shard_map/ppermute | solution.py:17
  50.6 7.7 %collective-permute-start.5 = (bf16[256,256]{1,0:T(8,128)(2,1)S(1)}, bf16[256,256]{1,0:T(8,128)(2,1)S(1)}, u32[]{:S(2)}, u32[]{:S(2)}) collective-permute-start(bf16[256,256]{1,0:T(8,128)(2,1)S(1)} %collective-permute-done.4), channel_id=1, source_target_pairs={{0,4},{4,8},{8,12},{12,16},{16,20},{20,24},{24,28},{28,0},{1,5},{5... | collective-permute-start | bytes 393224 | tf_op jit(solution)/shard_map/ppermute | solution.py:17
  58.2 7.7 %collective-permute-start.6 = (bf16[256,256]{1,0:T(8,128)(2,1)S(1)}, bf16[256,256]{1,0:T(8,128)(2,1)S(1)}, u32[]{:S(2)}, u32[]{:S(2)}) collective-permute-start(bf16[256,256]{1,0:T(8,128)(2,1)S(1)} %collective-permute-done.5), channel_id=1, source_target_pairs={{0,4},{4,8},{8,12},{12,16},{16,20},{20,24},{24,28},{28,0},{1,5},{5... | collective-permute-start | bytes 393224 | tf_op jit(solution)/shard_map/ppermute | solution.py:17
  58.9 17.6 %copy-start.1 = (bf16[384,2048]{1,0:T(8,128)(2,1)S(1)}, bf16[384,2048]{1,0:T(8,128)(2,1)}, u32[]{:S(2)}) copy-start(bf16[384,2048]{1,0:T(8,128)(2,1)} %param.13) | copy-start | bytes 4718596
  58.9 17.6 %copy-start.4 = (f32[2048]{0:T(1024)S(1)}, f32[2048]{0:T(1024)}, u32[]{:S(2)}) copy-start(f32[2048]{0:T(1024)} %param.14) | copy-start | bytes 24580
  78.4 0.9 copy-start.3
  100.8 116.6 %all-gather.11.cloned.1.call-start = ((), (), s32[]{:S(2)}) async-start(), calls=%async_computation.5 | async-start | bytes 4718592 | tf_op jit(solution)/shard_map/all_gather | solution.py:117
  101.4 189.3 %all-gather.9.cloned.1.call-start = ((), (), s32[]{:S(2)}) async-start(), calls=%async_computation.4 | async-start | bytes 4718592 | tf_op jit(solution)/shard_map/all_gather | solution.py:105
  102.0 188.8 %copy-start.5 = (f32[2048]{0:T(1024)S(1)}, f32[2048]{0:T(1024)}, u32[]{:S(2)}) copy-start(f32[2048]{0:T(1024)} %param.23) | copy-start | bytes 24580
  102.0 223.6 %reduce-scatter.2.cloned.1.call-start = ((), (), s32[]{:S(2)}) async-start(), calls=%async_computation.6 | async-start | bytes 1966080 | tf_op jit(solution)/shard_map/reduce_scatter | solution.py:118
Sparse Core Ops, SparseCore 0:
  9.5 45.0 all-gather.4
  56.7 39.4 all-gather.6
  100.9 41.5 all-reduce.18
  144.5 72.8 all-gather.10
  219.4 71.3 all-gather.8
  299.0 26.5 reduce-scatter.1
